TPU v7x, 32 devices: a whole 2x2x4 slice. The times are simulated.
32 devices in a mesh: sp: 8 (over z, x), tp: 4 (over y, core).
Axes of the slice: x: 2, y: 2, z: 4, core: 2. Of those that a mesh axis runs over, the one named last changes fastest.
Arguments:
- prompt: bfloat16 [4, 4096, 4096], P(None, 'sp'), may hold values from -6 to 6
- key_weight: bfloat16 [4096, 1024], P(None, 'tp'), may hold values from -0.09375 to 0.09375
- value_weight: bfloat16 [4096, 2048], P(None, 'tp'), may hold values from -0.09375 to 0.09375
- input_gate_weight: bfloat16 [4096, 16], P(None, 'tp'), may hold values from -0.09375 to 0.09375
- forget_gate_weight: bfloat16 [4096, 16], P(None, 'tp'), may hold values from -0.09375 to 0.09375
- forget_bias: float32 [16], P('tp'), may hold values from 3 to 11
- key_taps: bfloat16 [3, 1024], P(None, 'tp'), may hold values from -3 to 3
- extra_decay: float32 [4, 4096, 16], P(None, 'sp', 'tp'), may hold values from -1.5 to 0
- new_query: bfloat16 [4, 16, 64], P(None, 'tp'), may hold values from -6 to 6
- new_key: bfloat16 [4, 16, 64], P(None, 'tp'), may hold values from -6 to 6
- new_value: bfloat16 [4, 16, 128], P(None, 'tp', 'sp'), may hold values from -6 to 6
- new_input_gate: float32 [4, 16], P(None, 'tp'), may hold values from 2 to 7
- new_forget_gate: float32 [4, 16], P(None, 'tp'), may hold values from -2 to 4
- out_weight: bfloat16 [16, 128, 4096], P('tp', 'sp'), may hold values from -0.125 to 0.125
Outputs:
- cache_memory: bfloat16 [4, 16, 64, 128], P(None, 'tp', None, 'sp')
- cache_norm: bfloat16 [4, 16, 64], P(None, 'tp', 'sp')
- cache_peak: float32 [4, 16], P(None, 'tp')
- read_out: bfloat16 [4, 4096], P(None, ('sp', 'tp'))
All inputs are finite; a program needn't handle non-finite values.
Results may differ from a plain program's by a relative error of at most 0.012.
The roundings to bfloat16 on the way count: a program that leaves them out, or rounds other values in their place, can miss the bound.
Values may be sent and summed in bfloat16 or wider, within the bound.
A program may use at most 64 MiB of HBM per device.

v0:
```python
import jax
import jax.numpy as jnp
from jax import lax
from jax.sharding import PartitionSpec as P

KEY_DIM = 64


def with_halo(shard, sides, width):
    for axis, dim in sides:
        devices, length = (lax.axis_size(axis), shard.shape[dim])
        up = [(i, (i + 1) % devices) for i in range(devices - 1)]
        down = [(j, i) for i, j in up]
        last = lax.slice_in_dim(shard, length - width, length, axis=dim)
        leading = lax.slice_in_dim(shard, 0, width, axis=dim)
        before = lax.ppermute(last, axis, up)
        after = lax.ppermute(leading, axis, down)
        shard = jnp.concatenate([before, shard, after], axis=dim)
    return shard


def carried_in(shard, axis, combine, identity):
    devices, here = (lax.axis_size(axis), lax.axis_index(axis))
    everything = lax.all_gather(shard, axis)
    start = jnp.broadcast_to(jnp.asarray(identity, shard.dtype), shard.shape)

    def hop(k, before):
        at = devices - 1 - k
        reached = at > here
        new = combine(before, everything[at])
        return jnp.where(reached, new, before)

    return lax.fori_loop(0, devices, hop, start)


def widen(rounded):
    return lax.optimization_barrier(rounded).astype(jnp.float32)


def project(seq_rows, key_weight, value_weight, input_gate_weight, forget_gate_weight):
    seq_count, pos_count, width = seq_rows.shape
    flat_rows = seq_rows.reshape(seq_count * pos_count, width)
    key_raw = jnp.dot(flat_rows, key_weight, preferred_element_type=jnp.float32).astype(
        jnp.bfloat16
    )
    values = jnp.dot(flat_rows, value_weight, preferred_element_type=jnp.float32).astype(
        jnp.bfloat16
    )
    gate_weight = jnp.concatenate([input_gate_weight, forget_gate_weight], axis=1)
    gate_pre = jnp.dot(flat_rows, gate_weight, preferred_element_type=jnp.float32).astype(
        jnp.bfloat16
    )
    return (
        key_raw.reshape(seq_count, pos_count, -1),
        values.reshape(seq_count, pos_count, -1),
        gate_pre.reshape(seq_count, pos_count, -1),
    )


def key_conv(padded, key_taps):
    tap_f32 = key_taps.astype(jnp.float32)
    mixed = tap_f32[0] * padded[:, :-2] + tap_f32[1] * padded[:, 1:-1] + tap_f32[2] * padded[:, 2:]
    return (jax.nn.silu(mixed) * KEY_DIM ** (-0.5)).astype(jnp.bfloat16)


def gate_parts(gate_pre, forget_bias, extra):
    head_count = extra.shape[-1]
    gate_f32 = widen(gate_pre)
    input_pre = gate_f32[..., :head_count]
    log_forget = jax.nn.log_sigmoid(gate_f32[..., head_count:] + forget_bias) + extra
    return (input_pre, log_forget)


def suffix_of(log_forget):
    return jnp.sum(log_forget, axis=1, keepdims=True) - jnp.cumsum(log_forget, axis=1)


def add_later(earlier, latter):
    return earlier + latter


def body(
    prompt,
    key_weight,
    value_weight,
    input_gate_weight,
    forget_gate_weight,
    forget_bias,
    key_taps,
    extra_decay,
    new_query,
    new_key,
    new_value,
    new_input_gate,
    new_forget_gate,
    out_weight,
):
    seq_count = prompt.shape[0]
    head_count = extra_decay.shape[-1]
    key_size = new_key.shape[2]
    sp_count = lax.axis_size("sp")
    sp_index = lax.axis_index("sp")
    key_cols = key_size // sp_count
    key_raw, values, gate_pre = project(
        prompt, key_weight, value_weight, input_gate_weight, forget_gate_weight
    )
    input_pre, log_forget = gate_parts(gate_pre, forget_bias, extra_decay)
    padded = with_halo(key_raw, (("sp", 1),), 1)
    key_rows = key_conv(padded, key_taps)
    seg_total = jnp.sum(log_forget, axis=1)
    later_sum = carried_in(seg_total, "sp", add_later, jnp.zeros_like(seg_total))
    gate_log = input_pre + suffix_of(log_forget) + later_sum[:, None, :]
    peak_log = lax.pmax(jnp.max(gate_log, axis=1), "sp")
    scale = jnp.exp(gate_log - peak_log[:, None, :])
    pos_count = scale.shape[1]
    key_quartet = key_rows.reshape(seq_count, pos_count, head_count, key_size)
    value_four = values.reshape(seq_count, pos_count, head_count, -1)
    weighted_rows = (value_four * scale[..., None]).astype(jnp.bfloat16)
    memory_part = jnp.einsum(
        "slhk,slhv->shkv", key_quartet, weighted_rows, preferred_element_type=jnp.float32
    )
    normer_part = jnp.einsum(
        "slh,slhk->shk", scale, key_quartet.astype(jnp.float32), precision=lax.Precision.HIGHEST
    )
    memory_matrix, normer = (
        lax.psum_scatter(memory_part, "sp", scatter_dimension=3, tiled=True),
        lax.psum_scatter(normer_part, "sp", scatter_dimension=2, tiled=True),
    )
    forget_new = jax.nn.log_sigmoid(new_forget_gate)
    new_peak = jnp.maximum(forget_new + peak_log, new_input_gate)
    old_scale = jnp.exp(forget_new + peak_log - new_peak)
    new_scale = jnp.exp(new_input_gate - new_peak)
    key_new = new_key.astype(jnp.float32)
    key_new_slice = lax.dynamic_slice_in_dim(key_new, sp_index * key_cols, key_cols, 2)
    value_new = new_value.astype(jnp.float32)
    memory_next = (
        old_scale[:, :, None, None] * memory_matrix
        + new_scale[:, :, None, None] * key_new[:, :, :, None] * value_new[:, :, None, :]
    )
    normer_next = old_scale[:, :, None] * normer + new_scale[:, :, None] * key_new_slice
    query = new_query.astype(jnp.float32)
    query_slice = lax.dynamic_slice_in_dim(query, sp_index * key_cols, key_cols, 2)
    numer = jnp.sum(query[:, :, :, None] * memory_next, axis=2)
    denom = lax.psum(jnp.sum(query_slice * normer_next, axis=-1), "sp")
    read = (numer / jnp.maximum(jnp.abs(denom), 1.0)[:, :, None]).astype(jnp.bfloat16)
    partial_value = jnp.einsum("shv,hvd->sd", read, out_weight, preferred_element_type=jnp.float32)
    read_out = lax.psum_scatter(
        partial_value, ("sp", "tp"), scatter_dimension=1, tiled=True
    ).astype(jnp.bfloat16)
    return (memory_matrix.astype(jnp.bfloat16), normer.astype(jnp.bfloat16), peak_log, read_out)


def solution(mesh):
    placed = (
        P(None, "sp", None),
        P(None, "tp"),
        P(None, "tp"),
        P(None, "tp"),
        P(None, "tp"),
        P("tp"),
        P(None, "tp"),
        P(None, "sp", "tp"),
        P(None, "tp", None),
        P(None, "tp", None),
        P(None, "tp", "sp"),
        P(None, "tp"),
        P(None, "tp"),
        P("tp", "sp", None),
    )
    return jax.shard_map(
        body,
        mesh=mesh,
        in_specs=placed,
        out_specs=(
            P(None, "tp", None, "sp"),
            P(None, "tp", "sp"),
            P(None, "tp"),
            P(None, ("sp", "tp")),
        ),
        check_vma=False,
    )
```

profile of v0, /device:TPU:0, one launch (start us, length us, event | category | flops | bytes accessed | tf_op | source)
XLA Modules:
  0.0 337.2 jit_solution(1434747323576599410)
XLA Ops:
  7.2 1.5 copy-done
  8.8 8.2 %convolution_convert_fusion.1 = bf16[2048,256]{1,0:T(8,128)(2,1)S(1)} fusion(bf16[2048,4096]{1,0:T(8,128)(2,1)} %bitcast.42, bf16[4096,256]{1,0:T(8,128)(2,1)S(1)} %copy-done), kind=kOutput, calls=%fused_computation.5 | convolution fusion | flops 4295491584 | bytes 19922944 | tf_op jit(solution)/shard_map/dot_general | solution.py:43
  17.0 1.1 copy-done.2
  18.1 1.3 collective-permute-start.1
  19.4 5.5 %collective-permute-start = (bf16[4,1,256]{2,1,0:T(2,128)(2,1)S(1)}, bf16[4,1,256]{2,1,0:T(2,128)(2,1)S(1)}, u32[]{:S(2)}, u32[]{:S(2)}) collective-permute-start(bf16[4,1,256]{2,1,0:T(2,128)(2,1)S(1)} %get-tuple-element.140), channel_id=1, source_target_pairs={{0,4},{4,8},{8,12},{12,16},{16,20},{20,24},{24,28},{1,5},{5,9},{9,... | collective-permute-start | bytes 6152 | tf_op jit(solution)/shard_map/ppermute | solution.py:16
  25.0 10.2 %convolution_convert_fusion.2 = bf16[8,2048]{1,0:T(8,128)(2,1)S(1)} fusion(bf16[2048,4096]{1,0:T(8,128)(2,1)} %bitcast.43, bf16[4096,4]{0,1:T(4,128)(2,1)S(1)} %copy-done.3, bf16[4096,4]{0,1:T(4,128)(2,1)S(1)} %copy-done.4), kind=kOutput, calls=%fused_computation.6 | convolution fusion | flops 134365184 | bytes 16875520 | tf_op jit(solution)/shard_map/dot_general | solution.py:50
  35.2 0.2 fusion.19
  35.4 27.0 %all-gather.1 = f32[8,4,4]{2,1,0:T(4,128)S(1)} all-gather(f32[1,4,4]{2,1,0:T(4,128)S(1)} %bitcast.53), channel_id=2, replica_groups=mesh['sp'=8,'tp'=4] {'sp'}, dimensions={0}, use_global_device_ids=true | all-gather | bytes 576 | tf_op jit(solution)/shard_map/all_gather | solution.py:24
  62.4 0.3 while.16
  62.7 4.8 %reduce-window.6 = f32[4,4,4,128]{3,2,1,0:T(4,128)S(1)} reduce-window(f32[4,4,4,128]{3,2,1,0:T(4,128)S(1)} %reshape.55, f32[]{:T(128)} %constant.67.clone.1), window={size=1x1x1x128 pad=0_0x0_0x0_0x127_0}, to_apply=%region_1.2 | reduce-window | flops 1040384 | bytes 65540 | tf_op jit(solution)/shard_map/reduce-window
  67.6 0.2 slice_reduce_fusion
  67.8 0.7 reduce-window.9
  68.6 0.2 fusion.18
  68.7 14.8 %fusion = f32[2048,512]{1,0:T(8,128)} fusion(bf16[2048,4096]{1,0:T(8,128)(2,1)} %bitcast.44, bf16[4096,512]{1,0:T(8,128)(2,1)} %param.18), kind=kOutput, calls=%fused_computation.4 | convolution fusion | flops 8592031744 | bytes 25165824 | tf_op jit(solution)/shard_map/dot_general | solution.py:46
  83.6 19.5 %pmax.7 = f32[4,4]{1,0:T(4,128)S(1)} all-reduce(f32[4,4]{1,0:T(4,128)S(1)} %fusion.18), channel_id=1, replica_groups=mesh['sp'=8,'tp'=4] {'sp'}, use_global_device_ids=true, to_apply=%region_6.7 | all-reduce | flops 16 | bytes 128 | tf_op jit(solution)/shard_map/pmax | solution.py:113
  103.1 0.1 subtract_exponential_fusion
  103.2 5.2 %reshape.57 = f32[4,512,4,128]{3,2,1,0:T(4,128)} reshape(f32[2048,512]{1,0:T(8,128)} %fusion) | data formatting | bytes 8388608 | tf_op jit(solution)/shard_map/convert_element_type | solution.py:118
  108.5 5.2 %copy.23 = f32[4,512,4,128]{1,3,2,0:T(8,128)} copy(f32[4,512,4,128]{3,2,1,0:T(4,128)} %reshape.57) | data formatting | bytes 8388608 | tf_op jit(solution)/shard_map/convert_element_type | solution.py:118
  113.7 3.7 %multiply_convert_fusion.2 = bf16[4,512,256]{2,1,0:T(8,128)(2,1)S(1)} fusion(bf16[4,512,256]{2,1,0:T(8,128)(2,1)} %bitcast.48, bf16[4,1,256]{2,1,0:T(2,128)(2,1)S(1)} %collective-permute-done.1, bf16[4,1,256]{2,1,0:T(2,128)(2,1)S(1)} %collective-permute-done, f32[256]{0:T(256)S(1)} %bitcast.58, f32[256]{0:T(256)S(1)} %bitcast.57, f32[256]{0:T(256)S(1)} %bitcast.56), kind=kLoop, calls=%fused_computation.9 | loop fusion | flops 10485760 | bytes 2104320 | tf_op jit(solution)/shard_map/convert_element_type | solution.py:63
  117.4 1.3 copy.22
  118.8 4.3 %fusion.1 = f32[4,4,64,128]{2,3,1,0:T(8,128)} fusion(bf16[4,512,4,64]{1,3,2,0:T(8,128)(2,1)} %bitcast.45, f32[4,512,4,128]{1,3,2,0:T(8,128)} %copy.23, f32[4,512,4]{1,2,0:T(4,128)S(1)} %subtract_exponential_fusion), kind=kOutput, calls=%fused_computation.7 | convolution fusion | flops 136314880 | bytes 5799936 | tf_op jit(solution)/shard_map/slhk,slhv->shkv/dot_general | solution.py:119
  123.3 0.6 dynamic-slice
  124.6 0.9 fusion.10
  125.5 17.6 %all-reduce = f32[4,4,64]{2,1,0:T(4,128)S(1)} all-reduce(f32[4,4,64]{2,1,0:T(4,128)S(1)} %bitcast.55), channel_id=4, replica_groups=mesh['sp'=8,'tp'=4] {'sp'}, use_global_device_ids=true, to_apply=%region_8.9.clone | all-reduce | flops 1024 | bytes 8192
  143.2 0.2 multiply_reduce_fusion.1
  143.4 19.2 %psum.7 = f32[4,4]{1,0:T(4,128)S(1)} all-reduce(f32[4,4]{1,0:T(4,128)S(1)} %multiply_reduce_fusion.1), channel_id=1, replica_groups=mesh['sp'=8,'tp'=4] {'sp'}, use_global_device_ids=true, to_apply=%region_11.12 | all-reduce | flops 16 | bytes 128 | tf_op jit(solution)/shard_map/psum | solution.py:144
  162.6 22.6 %reduce-scatter.6.cloned.1.call-done = f32[4,4,64,16]{2,3,1,0:T(8,128)} async-done(((f32[4,4,64,128]{2,3,1,0:T(8,128)}), f32[4,4,64,16]{2,3,1,0:T(8,128)}) %reduce-scatter.6.cloned.1.call-update) | async-done | bytes 65552 | tf_op jit(solution)/shard_map/reduce_scatter | solution.py:126
  185.2 1.8 multiply_reduce_fusion
  187.0 4.1 %convolution_bitcast_fusion = f32[4096,4]{1,0:T(8,128)} fusion(bf16[4,16,4096]{2,1,0:T(8,128)(2,1)} %param.29, bf16[4,4,16]{2,1,0:T(4,128)(2,1)S(1)} %divide_convert_fusion), kind=kOutput, calls=%fused_computation.1 | convolution fusion | flops 2097152 | bytes 590336 | tf_op jit(solution)/shard_map/shv,hvd->sd/dot_general | solution.py:146
  191.2 0.7 dynamic-slice_convert_fusion
  191.8 137.0 %reduce-scatter.8.cloned.1.call-done = f32[128,4]{1,0:T(8,128)} async-done(((f32[4096,4]{1,0:T(8,128)}), f32[128,4]{1,0:T(8,128)}) %reduce-scatter.8.cloned.1.call-update) | async-done | bytes 2064
  328.9 1.5 copy.30
  (56 shorter events, 0.7 us)
Async XLA Ops:
  7.2 1.6 copy-start
  7.2 178.0 %reduce-scatter.6.cloned.1.call-start = ((), (), s32[]{:S(2)}) async-start(), calls=%async_computation.2 | async-start | bytes 1179648 | tf_op jit(solution)/shard_map/reduce_scatter | solution.py:126
  8.8 16.2 %copy-start.3 = (bf16[4096,4]{0,1:T(4,128)(2,1)S(1)}, bf16[4096,4]{0,1:T(4,128)(2,1)}, u32[]{:S(2)}) copy-start(bf16[4096,4]{0,1:T(4,128)(2,1)} %param.20) | copy-start | bytes 98308
  8.8 16.2 %copy-start.4 = (bf16[4096,4]{0,1:T(4,128)(2,1)S(1)}, bf16[4096,4]{0,1:T(4,128)(2,1)}, u32[]{:S(2)}) copy-start(bf16[4096,4]{0,1:T(4,128)(2,1)} %param.19) | copy-start | bytes 98308
  17.0 1.1 copy-start.2
  18.1 95.6 %collective-permute-start.1 = (bf16[4,1,256]{2,1,0:T(2,128)(2,1)S(1)}, bf16[4,1,256]{2,1,0:T(2,128)(2,1)S(1)}, u32[]{:S(2)}, u32[]{:S(2)}) collective-permute-start(bf16[4,1,256]{2,1,0:T(2,128)(2,1)S(1)} %get-tuple-element.141), channel_id=1, source_target_pairs={{4,0},{8,4},{12,8},{16,12},{20,16},{24,20},{28,24},{5,1},{9,5},{13... | collective-permute-start | bytes 6152 | tf_op jit(solution)/shard_map/ppermute | solution.py:17
  19.4 94.3 %collective-permute-start = (bf16[4,1,256]{2,1,0:T(2,128)(2,1)S(1)}, bf16[4,1,256]{2,1,0:T(2,128)(2,1)S(1)}, u32[]{:S(2)}, u32[]{:S(2)}) collective-permute-start(bf16[4,1,256]{2,1,0:T(2,128)(2,1)S(1)} %get-tuple-element.140), channel_id=1, source_target_pairs={{0,4},{4,8},{8,12},{12,16},{16,20},{20,24},{24,28},{1,5},{5,9},{9,... | collective-permute-start | bytes 6152 | tf_op jit(solution)/shard_map/ppermute | solution.py:16
  24.9 10.2 %copy-start.5 = (f32[4,512,4]{1,2,0:T(4,128)S(1)}, f32[4,512,4]{1,2,0:T(4,128)}, u32[]{:S(2)}) copy-start(f32[4,512,4]{1,2,0:T(4,128)} %param.23) | copy-start | bytes 98308
  25.0 10.2 %copy-start.13 = (f32[4]{0:T(128)S(1)}, f32[4]{0:T(128)}, u32[]{:S(2)}) copy-start(f32[4]{0:T(128)} %param.21) | copy-start | bytes 52
  68.7 34.5 %copy-start.8 = (bf16[3,256]{1,0:T(4,128)(2,1)S(1)}, bf16[3,256]{1,0:T(4,128)(2,1)}, u32[]{:S(2)}) copy-start(bf16[3,256]{1,0:T(4,128)(2,1)} %param.22) | copy-start | bytes 4612
  103.1 21.4 %copy-start.6 = (f32[4,4]{1,0:T(4,128)}, f32[4,4]{1,0:T(4,128)S(1)}, u32[]{:S(2)}) copy-start(f32[4,4]{1,0:T(4,128)S(1)} %pmax.7) | copy-start | bytes 196
  118.8 4.4 %copy-start.9 = (bf16[4,4,64]{2,1,0:T(4,128)(2,1)S(1)}, bf16[4,4,64]{2,1,0:T(4,128)(2,1)}, u32[]{:S(2)}) copy-start(bf16[4,4,64]{2,1,0:T(4,128)(2,1)} %param.24) | copy-start | bytes 6148
  118.8 4.4 %copy-start.7 = (bf16[4,4,64]{2,1,0:T(4,128)(2,1)S(1)}, bf16[4,4,64]{2,1,0:T(4,128)(2,1)}, u32[]{:S(2)}) copy-start(bf16[4,4,64]{2,1,0:T(4,128)(2,1)} %param.25) | copy-start | bytes 6148
  118.8 4.5 %copy-start.14 = (u32[32]{0:T(128)S(1)}, u32[32]{0:T(128)}, u32[]{:S(2)}) copy-start(u32[32]{0:T(128)} %constant.76) | copy-start | bytes 388
  118.8 5.7 %copy-start.11 = (f32[4,4]{1,0:T(4,128)S(1)}, f32[4,4]{1,0:T(4,128)}, u32[]{:S(2)}) copy-start(f32[4,4]{1,0:T(4,128)} %param.27) | copy-start | bytes 196
  118.8 5.7 %copy-start.12 = (f32[4,4]{1,0:T(4,128)S(1)}, f32[4,4]{1,0:T(4,128)}, u32[]{:S(2)}) copy-start(f32[4,4]{1,0:T(4,128)} %param.28) | copy-start | bytes 196
  118.8 5.8 %copy-start.1 = (bf16[4,512,256]{1,2,0:T(8,128)(2,1)S(1)}, bf16[4,512,256]{1,2,0:T(8,128)(2,1)}, u32[]{:S(2)}) copy-start(bf16[4,512,256]{1,2,0:T(8,128)(2,1)} %copy.22) | copy-start | bytes 3145732
  123.1 20.3 %copy-start.10 = (bf16[4,4,16]{2,1,0:T(4,128)(2,1)S(1)}, bf16[4,4,16]{2,1,0:T(4,128)(2,1)}, u32[]{:S(2)}) copy-start(bf16[4,4,16]{2,1,0:T(4,128)(2,1)} %param.26) | copy-start | bytes 1540
  123.1 205.7 %reduce-scatter.8.cloned.1.call-start = ((), (), s32[]{:S(2)}) async-start(), calls=%async_computation.3 | async-start | bytes 2162688
Sparse Core Ops, SparseCore 0:
  123.3 61.9 reduce-scatter.5
  191.3 137.5 reduce-scatter.7
where the time goes:
time: 338 us; the launch traced here: 337 us
  waiting for transfers between devices  160 us (47%)
  blocking collectives  83.3 us (25%)
  matrix products  42.6 us (13%)
  local copies, waits for them, and re-layouts  17.5 us (5%)
  between operations  15 us (4%)
  other arithmetic  12.1 us (4%)
  starting transfers between devices  6.87 us (2%)
    unnamed x3, waiting for transfers between devices  137 us
    all_gather x1, blocking collectives, carried_in(): everything = lax.all_gather(shard, axis)  27 us
    reduce_scatter x1, waiting for transfers between devices, body(): lax.psum_scatter(memory_part, 'sp', scatter_dimension=3, tiled=True)  22.6 us
    pmax x1, blocking collectives, body(): peak_log = lax.pmax(jnp.max(gate_log, axis=1), 'sp')  19.5 us
    psum x1, blocking collectives, body(): denom = lax.psum(jnp.sum(query_slice * normer_next, axis=-1), 'sp')  19.2 us
    unnamed x1, blocking collectives  17.6 us
    dot_general x1, matrix products, project(): jnp.dot(flat_rows, value_weight, preferred_element_type=jnp.float32)  14.8 us
    convert_element_type x2, local copies, waits for them, and re-layouts, body(): weighted_rows = (value_four * scale[..., None]).astype(jnp.bfloat16)  10.5 us
  transfers between devices with their start and end apart: 4, of which 2 were waited for; matrix products, arithmetic and copies ran while one was open for 13% of the time, Pallas kernels for 0%

commit v1 on v0

--- a/solution.py
+++ b/solution.py
@@ -141,7 +141,7 @@
     query = new_query.astype(jnp.float32)
     query_slice = lax.dynamic_slice_in_dim(query, sp_index * key_cols, key_cols, 2)
     numer = jnp.sum(query[:, :, :, None] * memory_next, axis=2)
-    denom = lax.psum(jnp.sum(query_slice * normer_next, axis=-1), "sp")
+    denom = jnp.sum(lax.all_gather(jnp.sum(query_slice * normer_next, axis=-1), "sp"), axis=0)
     read = (numer / jnp.maximum(jnp.abs(denom), 1.0)[:, :, None]).astype(jnp.bfloat16)
     partial_value = jnp.einsum("shv,hvd->sd", read, out_weight, preferred_element_type=jnp.float32)
     read_out = lax.psum_scatter(

time: 338 us -> 338 us (level)
  blocking collectives: 83.3 us -> 90.3 us
  waiting for transfers between devices: 160 us -> 153 us
    all_gather x0 -> x1, blocking collectives: none -> 26.2 us  [body(): lax.all_gather(jnp.sum(query_slice * normer_next, axis=-1), 'sp')]
    psum x1 -> x0, blocking collectives: 19.2 us -> none  [body(): denom = lax.psum(jnp.sum(query_slice * normer_next, axis=-1), 'sp')]
    reduce_scatter x1, waiting for transfers between devices: 22.6 us -> 15.6 us  [body(): lax.psum_scatter(memory_part, 'sp', scatter_dimension=3, tiled=True)]
where the time goes in v1:
time: 338 us; the launch traced here: 337 us
  waiting for transfers between devices  153 us (45%)
  blocking collectives  90.3 us (27%)
  matrix products  42.6 us (13%)
  local copies, waits for them, and re-layouts  17.5 us (5%)
  between operations  15 us (4%)
  other arithmetic  12.1 us (4%)
  starting transfers between devices  6.87 us (2%)
    unnamed x3, waiting for transfers between devices  137 us
    all_gather x1, blocking collectives, carried_in(): everything = lax.all_gather(shard, axis)  27 us
    all_gather x1, blocking collectives, body(): lax.all_gather(jnp.sum(query_slice * normer_next, axis=-1), 'sp')  26.2 us
    pmax x1, blocking collectives, body(): peak_log = lax.pmax(jnp.max(gate_log, axis=1), 'sp')  19.5 us
    unnamed x1, blocking collectives  17.6 us
    reduce_scatter x1, waiting for transfers between devices, body(): lax.psum_scatter(memory_part, 'sp', scatter_dimension=3, tiled=True)  15.6 us
    dot_general x1, matrix products, project(): jnp.dot(flat_rows, value_weight, preferred_element_type=jnp.float32)  14.8 us
    convert_element_type x2, local copies, waits for them, and re-layouts, body(): weighted_rows = (value_four * scale[..., None]).astype(jnp.bfloat16)  10.5 us
  transfers between devices with their start and end apart: 4, of which 2 were waited for; matrix products, arithmetic and copies ran while one was open for 13% of the time, Pallas kernels for 0%

profile of v1, /device:TPU:0, one launch (start us, length us, event | category | flops | bytes accessed | tf_op | source)
XLA Modules:
  0.0 337.2 jit_solution(16985457034822607928)
XLA Ops:
  7.2 1.5 copy-done
  8.8 8.2 %convolution_convert_fusion.1 = bf16[2048,256]{1,0:T(8,128)(2,1)S(1)} fusion(bf16[2048,4096]{1,0:T(8,128)(2,1)} %bitcast.43, bf16[4096,256]{1,0:T(8,128)(2,1)S(1)} %copy-done), kind=kOutput, calls=%fused_computation.5 | convolution fusion | flops 4295491584 | bytes 19922944 | tf_op jit(solution)/shard_map/dot_general | solution.py:43
  17.0 1.1 copy-done.2
  18.1 1.3 collective-permute-start.1
  19.4 5.5 %collective-permute-start = (bf16[4,1,256]{2,1,0:T(2,128)(2,1)S(1)}, bf16[4,1,256]{2,1,0:T(2,128)(2,1)S(1)}, u32[]{:S(2)}, u32[]{:S(2)}) collective-permute-start(bf16[4,1,256]{2,1,0:T(2,128)(2,1)S(1)} %get-tuple-element.140), channel_id=1, source_target_pairs={{0,4},{4,8},{8,12},{12,16},{16,20},{20,24},{24,28},{1,5},{5,9},{9,... | collective-permute-start | bytes 6152 | tf_op jit(solution)/shard_map/ppermute | solution.py:16
  25.0 10.2 %convolution_convert_fusion.2 = bf16[8,2048]{1,0:T(8,128)(2,1)S(1)} fusion(bf16[2048,4096]{1,0:T(8,128)(2,1)} %bitcast.44, bf16[4096,4]{0,1:T(4,128)(2,1)S(1)} %copy-done.3, bf16[4096,4]{0,1:T(4,128)(2,1)S(1)} %copy-done.4), kind=kOutput, calls=%fused_computation.6 | convolution fusion | flops 134365184 | bytes 16875520 | tf_op jit(solution)/shard_map/dot_general | solution.py:50
  35.2 0.2 fusion.19
  35.4 27.0 %all-gather.2 = f32[8,4,4]{2,1,0:T(4,128)S(1)} all-gather(f32[1,4,4]{2,1,0:T(4,128)S(1)} %bitcast.54), channel_id=2, replica_groups=mesh['sp'=8,'tp'=4] {'sp'}, dimensions={0}, use_global_device_ids=true | all-gather | bytes 576 | tf_op jit(solution)/shard_map/all_gather | solution.py:24
  62.4 0.3 while.16
  62.7 4.8 %reduce-window.6 = f32[4,4,4,128]{3,2,1,0:T(4,128)S(1)} reduce-window(f32[4,4,4,128]{3,2,1,0:T(4,128)S(1)} %reshape.58, f32[]{:T(128)} %constant.67.clone.1), window={size=1x1x1x128 pad=0_0x0_0x0_0x127_0}, to_apply=%region_1.2 | reduce-window | flops 1040384 | bytes 65540 | tf_op jit(solution)/shard_map/reduce-window
  67.6 0.2 slice_reduce_fusion
  67.8 0.7 reduce-window.9
  68.6 0.2 fusion.18
  68.7 14.8 %fusion = f32[2048,512]{1,0:T(8,128)} fusion(bf16[2048,4096]{1,0:T(8,128)(2,1)} %bitcast.45, bf16[4096,512]{1,0:T(8,128)(2,1)} %param.18), kind=kOutput, calls=%fused_computation.4 | convolution fusion | flops 8592031744 | bytes 25165824 | tf_op jit(solution)/shard_map/dot_general | solution.py:46
  83.6 19.5 %pmax.7 = f32[4,4]{1,0:T(4,128)S(1)} all-reduce(f32[4,4]{1,0:T(4,128)S(1)} %fusion.18), channel_id=1, replica_groups=mesh['sp'=8,'tp'=4] {'sp'}, use_global_device_ids=true, to_apply=%region_6.7 | all-reduce | flops 16 | bytes 128 | tf_op jit(solution)/shard_map/pmax | solution.py:113
  103.1 0.1 subtract_exponential_fusion
  103.2 5.2 %reshape.60 = f32[4,512,4,128]{3,2,1,0:T(4,128)} reshape(f32[2048,512]{1,0:T(8,128)} %fusion) | data formatting | bytes 8388608 | tf_op jit(solution)/shard_map/convert_element_type | solution.py:118
  108.5 5.2 %copy.23 = f32[4,512,4,128]{1,3,2,0:T(8,128)} copy(f32[4,512,4,128]{3,2,1,0:T(4,128)} %reshape.60) | data formatting | bytes 8388608 | tf_op jit(solution)/shard_map/convert_element_type | solution.py:118
  113.7 3.7 %multiply_convert_fusion.2 = bf16[4,512,256]{2,1,0:T(8,128)(2,1)S(1)} fusion(bf16[4,512,256]{2,1,0:T(8,128)(2,1)} %bitcast.49, bf16[4,1,256]{2,1,0:T(2,128)(2,1)S(1)} %collective-permute-done.1, bf16[4,1,256]{2,1,0:T(2,128)(2,1)S(1)} %collective-permute-done, f32[256]{0:T(256)S(1)} %bitcast.60, f32[256]{0:T(256)S(1)} %bitcast.59, f32[256]{0:T(256)S(1)} %bitcast.58), kind=kLoop, calls=%fused_computation.9 | loop fusion | flops 10485760 | bytes 2104320 | tf_op jit(solution)/shard_map/convert_element_type | solution.py:63
  117.4 1.3 copy.22
  118.8 4.3 %fusion.1 = f32[4,4,64,128]{2,3,1,0:T(8,128)} fusion(bf16[4,512,4,64]{1,3,2,0:T(8,128)(2,1)} %bitcast.46, f32[4,512,4,128]{1,3,2,0:T(8,128)} %copy.23, f32[4,512,4]{1,2,0:T(4,128)S(1)} %subtract_exponential_fusion), kind=kOutput, calls=%fused_computation.7 | convolution fusion | flops 136314880 | bytes 5799936 | tf_op jit(solution)/shard_map/slhk,slhv->shkv/dot_general | solution.py:119
  123.3 0.6 dynamic-slice
  124.7 0.9 fusion.10
  125.6 17.6 %all-reduce = f32[4,4,64]{2,1,0:T(4,128)S(1)} all-reduce(f32[4,4,64]{2,1,0:T(4,128)S(1)} %bitcast.57), channel_id=5, replica_groups=mesh['sp'=8,'tp'=4] {'sp'}, use_global_device_ids=true, to_apply=%region_8.9.clone | all-reduce | flops 1024 | bytes 8192
  143.2 0.2 multiply_reduce_fusion.1
  143.4 26.2 %all-gather.3 = f32[8,4,4]{2,1,0:T(4,128)S(1)} all-gather(f32[1,4,4]{2,1,0:T(4,128)S(1)} %bitcast.56), channel_id=3, replica_groups=mesh['sp'=8,'tp'=4] {'sp'}, dimensions={0}, use_global_device_ids=true | all-gather | bytes 576 | tf_op jit(solution)/shard_map/all_gather | solution.py:144
  169.6 15.6 %reduce-scatter.6.cloned.1.call-done = f32[4,4,64,16]{2,3,1,0:T(8,128)} async-done(((f32[4,4,64,128]{2,3,1,0:T(8,128)}), f32[4,4,64,16]{2,3,1,0:T(8,128)}) %reduce-scatter.6.cloned.1.call-update) | async-done | bytes 65552 | tf_op jit(solution)/shard_map/reduce_scatter | solution.py:126
  185.2 1.8 multiply_reduce_fusion
  187.0 4.1 %convolution_bitcast_fusion = f32[4096,4]{1,0:T(8,128)} fusion(bf16[4,16,4096]{2,1,0:T(8,128)(2,1)} %param.29, bf16[4,4,16]{2,1,0:T(4,128)(2,1)S(1)} %divide_convert_fusion), kind=kOutput, calls=%fused_computation.1 | convolution fusion | flops 2097152 | bytes 590336 | tf_op jit(solution)/shard_map/shv,hvd->sd/dot_general | solution.py:146
  191.2 0.7 dynamic-slice_convert_fusion
  191.9 137.0 %reduce-scatter.8.cloned.1.call-done = f32[128,4]{1,0:T(8,128)} async-done(((f32[4096,4]{1,0:T(8,128)}), f32[128,4]{1,0:T(8,128)}) %reduce-scatter.8.cloned.1.call-update) | async-done | bytes 2064
  328.9 1.5 copy.30
  (57 shorter events, 0.7 us)
Async XLA Ops:
  7.2 1.6 copy-start
  7.2 178.0 %reduce-scatter.6.cloned.1.call-start = ((), (), s32[]{:S(2)}) async-start(), calls=%async_computation.2 | async-start | bytes 1179648 | tf_op jit(solution)/shard_map/reduce_scatter | solution.py:126
  8.8 16.2 %copy-start.3 = (bf16[4096,4]{0,1:T(4,128)(2,1)S(1)}, bf16[4096,4]{0,1:T(4,128)(2,1)}, u32[]{:S(2)}) copy-start(bf16[4096,4]{0,1:T(4,128)(2,1)} %param.20) | copy-start | bytes 98308
  8.8 16.2 %copy-start.4 = (bf16[4096,4]{0,1:T(4,128)(2,1)S(1)}, bf16[4096,4]{0,1:T(4,128)(2,1)}, u32[]{:S(2)}) copy-start(bf16[4096,4]{0,1:T(4,128)(2,1)} %param.19) | copy-start | bytes 98308
  17.0 1.1 copy-start.2
  18.1 95.6 %collective-permute-start.1 = (bf16[4,1,256]{2,1,0:T(2,128)(2,1)S(1)}, bf16[4,1,256]{2,1,0:T(2,128)(2,1)S(1)}, u32[]{:S(2)}, u32[]{:S(2)}) collective-permute-start(bf16[4,1,256]{2,1,0:T(2,128)(2,1)S(1)} %get-tuple-element.141), channel_id=1, source_target_pairs={{4,0},{8,4},{12,8},{16,12},{20,16},{24,20},{28,24},{5,1},{9,5},{13... | collective-permute-start | bytes 6152 | tf_op jit(solution)/shard_map/ppermute | solution.py:17
  19.4 94.3 %collective-permute-start = (bf16[4,1,256]{2,1,0:T(2,128)(2,1)S(1)}, bf16[4,1,256]{2,1,0:T(2,128)(2,1)S(1)}, u32[]{:S(2)}, u32[]{:S(2)}) collective-permute-start(bf16[4,1,256]{2,1,0:T(2,128)(2,1)S(1)} %get-tuple-element.140), channel_id=1, source_target_pairs={{0,4},{4,8},{8,12},{12,16},{16,20},{20,24},{24,28},{1,5},{5,9},{9,... | collective-permute-start | bytes 6152 | tf_op jit(solution)/shard_map/ppermute | solution.py:16
  24.9 10.2 %copy-start.5 = (f32[4,512,4]{1,2,0:T(4,128)S(1)}, f32[4,512,4]{1,2,0:T(4,128)}, u32[]{:S(2)}) copy-start(f32[4,512,4]{1,2,0:T(4,128)} %param.23) | copy-start | bytes 98308
  25.0 10.2 %copy-start.13 = (f32[4]{0:T(128)S(1)}, f32[4]{0:T(128)}, u32[]{:S(2)}) copy-start(f32[4]{0:T(128)} %param.21) | copy-start | bytes 52
  68.7 34.5 %copy-start.8 = (bf16[3,256]{1,0:T(4,128)(2,1)S(1)}, bf16[3,256]{1,0:T(4,128)(2,1)}, u32[]{:S(2)}) copy-start(bf16[3,256]{1,0:T(4,128)(2,1)} %param.22) | copy-start | bytes 4612
  103.1 21.4 %copy-start.6 = (f32[4,4]{1,0:T(4,128)}, f32[4,4]{1,0:T(4,128)S(1)}, u32[]{:S(2)}) copy-start(f32[4,4]{1,0:T(4,128)S(1)} %pmax.7) | copy-start | bytes 196
  118.8 4.4 %copy-start.9 = (bf16[4,4,16]{2,1,0:T(4,128)(2,1)S(1)}, bf16[4,4,16]{2,1,0:T(4,128)(2,1)}, u32[]{:S(2)}) copy-start(bf16[4,4,16]{2,1,0:T(4,128)(2,1)} %param.26) | copy-start | bytes 1540
  118.8 4.5 %copy-start.10 = (bf16[4,4,64]{2,1,0:T(4,128)(2,1)S(1)}, bf16[4,4,64]{2,1,0:T(4,128)(2,1)}, u32[]{:S(2)}) copy-start(bf16[4,4,64]{2,1,0:T(4,128)(2,1)} %param.24) | copy-start | bytes 6148
  118.8 4.5 %copy-start.7 = (bf16[4,4,64]{2,1,0:T(4,128)(2,1)S(1)}, bf16[4,4,64]{2,1,0:T(4,128)(2,1)}, u32[]{:S(2)}) copy-start(bf16[4,4,64]{2,1,0:T(4,128)(2,1)} %param.25) | copy-start | bytes 6148
  118.8 4.5 %copy-start.14 = (u32[32]{0:T(128)S(1)}, u32[32]{0:T(128)}, u32[]{:S(2)}) copy-start(u32[32]{0:T(128)} %constant.76) | copy-start | bytes 388
  118.8 5.8 %copy-start.11 = (f32[4,4]{1,0:T(4,128)S(1)}, f32[4,4]{1,0:T(4,128)}, u32[]{:S(2)}) copy-start(f32[4,4]{1,0:T(4,128)} %param.27) | copy-start | bytes 196
  118.8 5.8 %copy-start.12 = (f32[4,4]{1,0:T(4,128)S(1)}, f32[4,4]{1,0:T(4,128)}, u32[]{:S(2)}) copy-start(f32[4,4]{1,0:T(4,128)} %param.28) | copy-start | bytes 196
  118.8 5.9 %copy-start.1 = (bf16[4,512,256]{1,2,0:T(8,128)(2,1)S(1)}, bf16[4,512,256]{1,2,0:T(8,128)(2,1)}, u32[]{:S(2)}) copy-start(bf16[4,512,256]{1,2,0:T(8,128)(2,1)} %copy.22) | copy-start | bytes 3145732
  123.1 205.7 %reduce-scatter.8.cloned.1.call-start = ((), (), s32[]{:S(2)}) async-start(), calls=%async_computation.3 | async-start | bytes 2162688
Sparse Core Ops, SparseCore 0:
  123.3 61.9 reduce-scatter.5
  191.3 137.5 reduce-scatter.7
